TPU v7x, 32 devices: a whole 2x2x4 slice. The times are simulated.
32 devices in a mesh: ep: 8 (over z, y), tp: 4 (over x, core).
Axes of the slice: x: 2, y: 2, z: 4, core: 2. Of those that a mesh axis runs over, the one named last changes fastest.
Arguments:
- queries: bfloat16 [1024, 512], P('ep', 'tp'), may hold values from -8 to 8
- key_cache: bfloat16 [4, 64, 1024], P('tp', None, 'ep'), may hold values from -4.5 to 4.5
- value_cache: bfloat16 [4, 64, 1024], P('tp', None, 'ep'), may hold values from -6 to 6
- cum_gate: float32 [4, 1024], P('tp'), may hold values from -256 to 0, as said below
- out_weight: bfloat16 [512, 2048], replicated, may hold values from -1 to 1
- routed_input: bfloat16 [2048, 2048], P('ep'), may hold values from -6 to 6
- norm_gain: bfloat16 [2048], replicated, may hold values from 0.099609375 to 1.8984375
- routes: int32 [2048, 2], P('ep'), may hold values from 0 to 7, all different within a row; in each aligned block of 64 rows (0 to 63, 64 to 127, ...) at most 24 rows name the same one
- route_weight: float32 [2048, 2], P('ep'), may hold values from 0.2 to 1
- expert_gate: bfloat16 [8, 2048, 1024], P('ep', None, 'tp'), may hold values from -0.125 to 0.125
- expert_up: bfloat16 [8, 2048, 1024], P('ep', None, 'tp'), may hold values from -0.125 to 0.125
- expert_down: bfloat16 [8, 1024, 2048], P('ep', 'tp'), may hold values from -0.1875 to 0.1875
Outputs:
- mixed_out: bfloat16 [1024, 2048], P(('ep', 'tp'))
- expert_out: bfloat16 [2048, 2048], P(('ep', 'tp'))
Inputs may be any that keep to these rules, and one draw needn't show every extreme that they name: `cum_gate`: Non-increasing along positions in every head. `routes`: each row names 2 different experts. In each aligned block of 64 rows (the rows of one device) no expert is named by more than 24 rows, a bound that some block reaches.
All inputs are finite; a program needn't handle non-finite values.
Results may differ from a plain program's by a relative error of at most 0.012.
Values may be sent and summed in bfloat16 or wider, within the bound.
A program may use at most 64 MiB of HBM per device.

v0:
```python
import jax
import jax.numpy as jnp
from jax import lax
from jax.sharding import PartitionSpec as P


def slot_chooser(route_rows, expert_count, capacity):
    token_rows, top_count = route_rows.shape
    flat = route_rows.reshape(token_rows * top_count)
    same = (flat[:, None] == jnp.arange(expert_count, dtype=jnp.int32)[None, :]).astype(jnp.int32)
    earlier = jnp.cumsum(same, axis=0) - same
    rank = jnp.sum(earlier * same, axis=1)
    slot = flat * capacity + rank
    chosen = slot[:, None] == jnp.arange(expert_count * capacity, dtype=jnp.int32)[None, :]
    return chosen.astype(jnp.bfloat16).reshape(token_rows, top_count, expert_count * capacity)


def rms_rows(source, norm_gain):
    widened = source.astype(jnp.float32)
    scale = lax.rsqrt(jnp.mean(widened * widened, axis=-1, keepdims=True) + 1e-06)
    return (widened * scale * norm_gain.astype(jnp.float32)).astype(jnp.bfloat16)


def mixer_half(queries, key_cache, value_cache, cum_gate, out_weight):
    seq_rows = queries.shape[0]
    local_heads = key_cache.shape[0]
    head_size = key_cache.shape[1]
    group = queries.shape[1] // (local_heads * head_size)
    own_start = lax.axis_index("ep") * seq_rows
    query_heads = queries.reshape(seq_rows, local_heads, group, head_size)
    query_pos = own_start + jnp.arange(seq_rows, dtype=jnp.int32)
    gate_query = lax.dynamic_slice_in_dim(cum_gate, own_start, seq_rows, 1)
    gate_rows = jnp.transpose(gate_query)[:, :, None, None]
    scale = head_size ** (-0.5)
    best_start = jnp.full((seq_rows, local_heads, group), -jnp.inf, jnp.float32)
    total_start = jnp.zeros((seq_rows, local_heads, group), jnp.float32)
    summed_start = jnp.zeros((seq_rows, local_heads * group * head_size), jnp.float32)
    pieces = (
        lax.all_gather(key_cache, "ep", axis=2, tiled=True),
        lax.all_gather(value_cache, "ep", axis=2, tiled=True),
    )

    def update(state):
        best, total, summed = state
        key_piece, value_piece = pieces
        width = key_piece.shape[2]
        scores = (
            jnp.einsum("thgd,hds->thgs", query_heads, key_piece, preferred_element_type=jnp.float32)
            * scale
        )
        scores = scores + gate_rows - cum_gate[None, :, None, :]
        key_pos = jnp.arange(width, dtype=jnp.int32)
        allowed = key_pos[None, :] <= query_pos[:, None]
        scores = jnp.where(allowed[:, None, None, :], scores, -jnp.inf)
        new_best = jnp.max(scores, axis=-1)
        factor = jnp.exp(best - new_best)
        weights = jnp.exp(scores - new_best[..., None])
        new_total = total * factor + jnp.sum(weights, axis=-1)
        product = jnp.einsum(
            "thgs,hds->thgd",
            weights.astype(jnp.bfloat16),
            value_piece,
            preferred_element_type=jnp.float32,
        )
        new_summed = summed.reshape(product.shape) * factor[..., None] + product
        return (new_best, new_total, new_summed.reshape(seq_rows, local_heads * group * head_size))

    best, total, summed = lax.cond(
        jnp.int32(0) <= own_start,
        update,
        lambda state: state,
        (best_start, total_start, summed_start),
    )
    attended = summed.reshape(seq_rows, local_heads, group, head_size) / total[..., None]
    attended = attended.astype(jnp.bfloat16).reshape(seq_rows, local_heads * group * head_size)
    by_position = lax.all_to_all(attended, "tp", split_axis=0, concat_axis=1, tiled=True)
    return jnp.dot(by_position, out_weight, preferred_element_type=jnp.float32).astype(jnp.bfloat16)


def expert_half(routed_input, norm_gain, routes, route_weight, expert_gate, expert_up, expert_down):
    group_size = lax.axis_size("tp")
    ep_size = lax.axis_size("ep")
    tp_index = lax.axis_index("tp")
    seq_rows, width = routed_input.shape
    own_rows = seq_rows // group_size
    local_experts = expert_gate.shape[0]
    expert_count = local_experts * ep_size
    top_count = routes.shape[1]
    capacity = max(2, own_rows * top_count * 3 // (2 * expert_count))
    per_device = local_experts * capacity
    mine = lax.dynamic_slice_in_dim(routed_input, tp_index * own_rows, own_rows, 0)
    own_routes = lax.dynamic_slice_in_dim(routes, tp_index * own_rows, own_rows, 0)
    chooser = slot_chooser(own_routes, expert_count, capacity)
    normed = rms_rows(mine, norm_gain)
    outgoing = jnp.einsum("tks,td->sd", chooser, normed, preferred_element_type=jnp.float32).astype(
        jnp.bfloat16
    )
    arrived = lax.all_to_all(
        outgoing.reshape(1, ep_size, per_device, width),
        "ep",
        split_axis=1,
        concat_axis=1,
        tiled=True,
    )
    received = lax.all_gather(arrived, "tp", axis=0, tiled=True)
    blocks = received.shape[0]
    divide_point = received.reshape(blocks, ep_size, local_experts, capacity, width)
    gate = jnp.einsum(
        "abecd,edf->abecf", divide_point, expert_gate, preferred_element_type=jnp.float32
    )
    upper = jnp.einsum(
        "abecd,edf->abecf", divide_point, expert_up, preferred_element_type=jnp.float32
    )
    hidden = (jax.nn.silu(gate) * upper).astype(jnp.bfloat16)
    partial_value = jnp.einsum(
        "abecf,efd->abecd", hidden, expert_down, preferred_element_type=jnp.float32
    )
    rounded = lax.optimization_barrier(partial_value.astype(jnp.bfloat16)).astype(jnp.float32)
    summed = lax.psum_scatter(
        rounded.reshape(lax.axis_size("tp") * 1, ep_size, per_device, width).astype(jnp.bfloat16),
        "tp",
        scatter_dimension=0,
        tiled=True,
    )
    returned = lax.all_to_all(summed, "ep", split_axis=1, concat_axis=1, tiled=True)
    picked = jnp.einsum(
        "tks,sd->tkd",
        chooser,
        returned.reshape(ep_size * per_device, width),
        preferred_element_type=jnp.float32,
    )
    own_weight = lax.dynamic_slice_in_dim(route_weight, tp_index * own_rows, own_rows, 0)
    return jnp.sum(own_weight[:, :, None] * picked, axis=1).astype(jnp.bfloat16)


def body(
    queries,
    key_cache,
    value_cache,
    cum_gate,
    out_weight,
    routed_input,
    norm_gain,
    routes,
    route_weight,
    expert_gate,
    expert_up,
    expert_down,
):
    mixed_out = mixer_half(queries, key_cache, value_cache, cum_gate, out_weight)
    expert_out = expert_half(
        routed_input, norm_gain, routes, route_weight, expert_gate, expert_up, expert_down
    )
    return (mixed_out, expert_out)


def solution(mesh):
    return jax.shard_map(
        body,
        mesh=mesh,
        in_specs=(
            P("ep", "tp"),
            P("tp", None, "ep"),
            P("tp", None, "ep"),
            P("tp", None),
            P(),
            P("ep", None),
            P(),
            P("ep", None),
            P("ep", None),
            P("ep", None, "tp"),
            P("ep", None, "tp"),
            P("ep", "tp", None),
        ),
        out_specs=(P(("ep", "tp"), None), P(("ep", "tp"), None)),
        check_vma=False,
    )
```

profile of v0, /device:TPU:0, one launch (start us, length us, event | category | flops | bytes accessed | tf_op | source)
XLA Modules:
  0.0 172.3 jit_solution(1201821751376832034)
XLA Ops:
  7.2 0.9 constant_dynamic-slice_fusion
  8.2 0.1 copy.56
  8.3 0.1 eq.51
  8.4 0.1 fusion.36
  8.5 0.2 reduce_window_sum.11
  8.7 0.2 select_reduce_fusion
  8.9 0.1 reduce_sum.48
  9.1 0.8 multiply_add_fusion
  9.8 0.1 convert_reduce_fusion
  9.9 1.1 fusion.23
  11.1 0.7 convert_element_type.68
  11.8 1.4 convolution_convert_fusion.1
  13.1 27.4 %all_to_all.29 = bf16[1,8,24,2048]{3,2,0,1:T(8,128)(2,1)} all-to-all(bf16[1,8,24,2048]{3,2,0,1:T(8,128)(2,1)S(1)} %bitcast.129), channel_id=1, replica_groups=mesh['ep'=8,'tp'=4] {'ep'}, dimensions={1} | all-to-all | bytes 1572864 | tf_op jit(solution)/shard_map/all_to_all | solution.py:98
  40.6 27.6 %all-gather.2.cloned.1.call-done = bf16[4,8,24,2048]{3,2,1,0:T(8,128)(2,1)} async-done(((bf16[1,8,24,2048]{3,2,1,0:T(8,128)(2,1)}), bf16[4,8,24,2048]{3,2,1,0:T(8,128)(2,1)}) %all-gather.2.cloned.1.call-update) | async-done | bytes 3145744 | tf_op jit(solution)/shard_map/all_gather | solution.py:105
  68.2 3.8 %convolution_bitcast_fusion.2 = f32[4,8,1,24,256]{4,3,1,0,2:T(8,128)} fusion(bf16[4,8,24,2048]{3,2,1,0:T(8,128)(2,1)} %all-gather.2.cloned.1.call-done, bf16[1,2048,256]{2,1,0:T(8,128)(2,1)S(1)} %copy-done.5), kind=kOutput, calls=%fused_computation.26 | convolution fusion | flops 805306368 | bytes 4980736 | tf_op jit(solution)/shard_map/abecd,edf->abecf/dot_general | solution.py:108
  72.0 7.9 %fusion.13 = bf16[4,8,1,24,2048]{4,3,1,0,2:T(8,128)(2,1)} fusion(bf16[1,256,2048]{2,1,0:T(8,128)(2,1)} %param.25, bf16[4,8,24,2048]{3,2,1,0:T(8,128)(2,1)} %all-gather.2.cloned.1.call-done, bf16[1,2048,256]{2,1,0:T(8,128)(2,1)} %param.24, f32[4,8,1,24,256]{4,3,1,0,2:T(8,128)} %convolution_bitcast_fusion.2), kind=kOutput, calls=%fused_computation.21 | convolution fusion | flops 1613365248 | bytes 9175040 | tf_op jit(solution)/shard_map/abecf,efd->abecd/dot_general | solution.py:115
  79.9 0.7 copy-done.2
  80.6 26.2 %all_gather.10 = bf16[1,64,1024]{2,1,0:T(8,128)(2,1)S(1)} all-gather(bf16[1,64,128]{2,1,0:T(8,128)(2,1)S(1)} %copy-done.2), channel_id=1, replica_groups=mesh['ep'=8,'tp'=4] {'ep'}, dimensions={2}, use_global_device_ids=true | all-gather | bytes 147456 | tf_op jit(solution)/shard_map/all_gather | solution.py:40
  106.7 26.2 %all_gather.9 = bf16[1,64,1024]{2,1,0:T(8,128)(2,1)S(1)} all-gather(bf16[1,64,128]{2,1,0:T(8,128)(2,1)S(1)} %copy-done.3), channel_id=1, replica_groups=mesh['ep'=8,'tp'=4] {'ep'}, dimensions={2}, use_global_device_ids=true | all-gather | bytes 147456 | tf_op jit(solution)/shard_map/all_gather | solution.py:39
  132.9 1.2 conditional.1
  132.9 0.1 dynamic-slice_bitcast_fusion
  133.0 0.1 iota_compare_fusion
  133.1 0.1 copy.53
  133.2 0.4 fusion.41
  133.7 0.2 fusion.7
  133.8 0.3 fusion.5
  134.2 0.1 copy.54
  134.3 6.3 %all_to_all.30 = bf16[4,32,128]{2,1,0:T(8,128)(2,1)S(1)} all-to-all(bf16[4,32,128]{2,1,0:T(8,128)(2,1)S(1)} %bitcast.133), channel_id=1, replica_groups=mesh['ep'=8,'tp'=4] {'tp'}, dimensions={0} | all-to-all | bytes 65536 | tf_op jit(solution)/shard_map/all_to_all | solution.py:76
  140.6 3.5 %all-to-all-start.2 = ((bf16[1,8,24,2048]{3,2,0,1:T(8,128)(2,1)}), bf16[1,8,24,2048]{3,2,0,1:T(8,128)(2,1)S(1)}, u32[]{:S(2)}, u32[]{:S(2)}) async-start(bf16[1,8,24,2048]{3,2,0,1:T(8,128)(2,1)} %bitcast.130), calls=%async_computation.3 | async-start | bytes 1572864 | tf_op jit(solution)/shard_map/all_to_all | solution.py:125
  144.2 1.1 convolution_convert_fusion.2
  145.4 19.1 %all-to-all-done.2 = bf16[1,8,24,2048]{3,2,0,1:T(8,128)(2,1)S(1)} async-done(((bf16[1,8,24,2048]{3,2,0,1:T(8,128)(2,1)}), bf16[1,8,24,2048]{3,2,0,1:T(8,128)(2,1)S(1)}, u32[]{:S(2)}, u32[]{:S(2)}) %all-to-all-start.2) | async-done | bytes 786464 | tf_op jit(solution)/shard_map/all_to_all | solution.py:125
  164.4 1.1 fusion.15
  (25 shorter events, 0.3 us)
Async XLA Ops:
  7.2 137.1 %copy-start = (bf16[512,2048]{1,0:T(8,128)(2,1)S(1)}, bf16[512,2048]{1,0:T(8,128)(2,1)}, u32[]{:S(2)}) copy-start(bf16[512,2048]{1,0:T(8,128)(2,1)} %param.18) | copy-start | bytes 6291460
  7.2 61.0 %copy-start.5 = (bf16[1,2048,256]{2,1,0:T(8,128)(2,1)S(1)}, bf16[1,2048,256]{2,1,0:T(8,128)(2,1)}, u32[]{:S(2)}) copy-start(bf16[1,2048,256]{2,1,0:T(8,128)(2,1)} %param.23) | copy-start | bytes 3145732
  7.2 61.0 %all-gather.2.cloned.1.call-start = ((), (), s32[]{:S(2)}) async-start(), calls=%async_computation.4 | async-start | bytes 3932160 | tf_op jit(solution)/shard_map/all_gather | solution.py:105
  40.5 100.0 %reduce-scatter.2.cloned.1.call-start = ((), (), s32[]{:S(2)}) async-start(), calls=%async_computation.5 | async-start | bytes 3932160 | tf_op jit(solution)/shard_map/reduce_scatter | solution.py:119
  79.8 0.7 copy-start.2
  79.8 26.9 %copy-start.3 = (bf16[1,64,128]{2,1,0:T(8,128)(2,1)S(1)}, bf16[1,64,128]{2,1,0:T(8,128)(2,1)}, u32[]{:S(2)}) copy-start(bf16[1,64,128]{2,1,0:T(8,128)(2,1)} %param.15) | copy-start | bytes 49156
  79.8 53.1 %copy-start.1 = (bf16[128,128]{1,0:T(8,128)(2,1)S(1)}, bf16[128,128]{1,0:T(8,128)(2,1)}, u32[]{:S(2)}) copy-start(bf16[128,128]{1,0:T(8,128)(2,1)} %param.14) | copy-start | bytes 98308
  79.8 53.1 %copy-start.6 = (f32[1,1024]{1,0:T(1,128)S(1)}, f32[1,1024]{1,0:T(1,128)}, u32[]{:S(2)}) copy-start(f32[1,1024]{1,0:T(1,128)} %param.17) | copy-start | bytes 12292
  132.9 11.2 %copy-start.4 = (f32[256,2]{0,1:T(2,128)S(1)}, f32[256,2]{0,1:T(2,128)}, u32[]{:S(2)}) copy-start(f32[256,2]{0,1:T(2,128)} %param.22) | copy-start | bytes 6148
  140.6 23.8 %all-to-all-start.2 = ((bf16[1,8,24,2048]{3,2,0,1:T(8,128)(2,1)}), bf16[1,8,24,2048]{3,2,0,1:T(8,128)(2,1)S(1)}, u32[]{:S(2)}, u32[]{:S(2)}) async-start(bf16[1,8,24,2048]{3,2,0,1:T(8,128)(2,1)} %bitcast.130), calls=%async_computation.3 | async-start | bytes 1572864 | tf_op jit(solution)/shard_map/all_to_all | solution.py:125
Sparse Core Ops, SparseCore 0:
  40.6 27.5 all-gather.1
  80.0 37.8 reduce-scatter.1
where the time goes:
time: 173 us; the launch traced here: 172 us
  blocking collectives  86 us (50%)
  waiting for transfers between devices  46.7 us (27%)
  matrix products  15.9 us (9%)
  between operations  14.2 us (8%)
  starting transfers between devices  3.63 us (2%)
  other arithmetic  3.38 us (2%)
  local copies, waits for them, and re-layouts  2.47 us (1%)
    all_gather x1, waiting for transfers between devices, expert_half(): received = lax.all_gather(arrived, 'tp', axis=0, tiled=True)  27.6 us
    all_to_all x1, blocking collectives, expert_half(): lax.all_to_all(outgoing.reshape(1, ep_size, per_device, width), 'ep', spl...  27.4 us
    all_gather x1, blocking collectives, mixer_half(): lax.all_gather(value_cache, 'ep', axis=2, tiled=True)  26.2 us
    all_gather x1, blocking collectives, mixer_half(): lax.all_gather(key_cache, 'ep', axis=2, tiled=True)  26.2 us
    all_to_all x1, waiting for transfers between devices, expert_half(): lax.all_to_all(summed, 'ep', split_axis=1, concat_axis=1, tiled=True)  19.1 us
    dot_general x1, matrix products, expert_half(): jnp.einsum('abecf,efd->abecd', hidden, expert_down, preferred_element_typ...  7.85 us
    all_to_all x1, blocking collectives, mixer_half(): lax.all_to_all(attended, 'tp', split_axis=0, concat_axis=1, tiled=True)  6.3 us
    dot_general x1, matrix products, expert_half(): jnp.einsum('abecd,edf->abecf', divide_point, expert_gate, preferred_eleme...  3.78 us
  transfers between devices with their start and end apart: 3, of which 2 were waited for; matrix products, arithmetic and copies ran while one was open for 1% of the time, Pallas kernels for 0%

commit v1 on v0

--- a/solution.py
+++ b/solution.py
@@ -95,13 +95,20 @@
     outgoing = jnp.einsum("tks,td->sd", chooser, normed, preferred_element_type=jnp.float32).astype(
         jnp.bfloat16
     )
-    arrived = lax.all_to_all(
-        outgoing.reshape(1, ep_size, per_device, width),
-        "ep",
-        split_axis=1,
-        concat_axis=1,
-        tiled=True,
-    )
+    array = outgoing.reshape(1, ep_size, per_device, width)
+    ways, here = (lax.axis_size("ep"), lax.axis_index("ep"))
+    width_2 = array.shape[1] // ways
+    shape = list(array.shape)
+    shape[1] = width_2
+    height = shape[1]
+    shape[1] = height * ways
+    full = jnp.zeros(shape, array.dtype)
+    for mask in range(ways):
+        part = lax.dynamic_slice_in_dim(array, (here ^ mask) * width_2, width_2, axis=1)
+        if mask:
+            part = lax.ppermute(part, "ep", [(d, d ^ mask) for d in range(ways)])
+        full = lax.dynamic_update_slice_in_dim(full, part, (here ^ mask) * height, axis=1)
+    arrived = full
     received = lax.all_gather(arrived, "tp", axis=0, tiled=True)
     blocks = received.shape[0]
     divide_point = received.reshape(blocks, ep_size, local_experts, capacity, width)

time: 173 us -> 172 us (level)
  blocking collectives: 86 us -> 58.6 us
  waiting for transfers between devices: 46.7 us -> 59.6 us
  starting transfers between devices: 3.63 us -> 16.2 us
    all_to_all x1 -> x0, blocking collectives: 27.4 us -> none  [expert_half(): lax.all_to_all(outgoing.reshape(1, ep_size, per_device, width), 'ep', spl...]
    ppermute x0 -> x7, starting transfers between devices: none -> 12.6 us  [expert_half(): part = lax.ppermute(part, 'ep', [(d, d ^ mask) for d in range(ways)])]
    ppermute x0 -> x7, waiting for transfers between devices: none -> 10.1 us  [expert_half(): part = lax.ppermute(part, 'ep', [(d, d ^ mask) for d in range(ways)])]
    all_gather x1, waiting for transfers between devices: 27.6 us -> 30.4 us  [expert_half(): received = lax.all_gather(arrived, 'tp', axis=0, tiled=True)]
  transfers between devices with their start and end apart: 3 -> 10, of which waited for: 2 -> 3; matrix products, arithmetic and copies ran while one was open for 1% -> 2% of each run, Pallas kernels for 0% -> 0%
where the time goes in v1:
time: 172 us
  waiting for transfers between devices  59.6 us (35%)
  blocking collectives  58.6 us (34%)
  starting transfers between devices  16.2 us (9%)
  matrix products  15.8 us (9%)
  between operations  14.3 us (8%)
  local copies, waits for them, and re-layouts  3.55 us (2%)
  other arithmetic  3.38 us (2%)
    all_gather x1, waiting for transfers between devices, expert_half(): received = lax.all_gather(arrived, 'tp', axis=0, tiled=True)  30.4 us
    all_gather x1, blocking collectives, mixer_half(): lax.all_gather(value_cache, 'ep', axis=2, tiled=True)  26.2 us
    all_gather x1, blocking collectives, mixer_half(): lax.all_gather(key_cache, 'ep', axis=2, tiled=True)  26.2 us
    all_to_all x1, waiting for transfers between devices, expert_half(): lax.all_to_all(summed, 'ep', split_axis=1, concat_axis=1, tiled=True)  19.1 us
    ppermute x7, starting transfers between devices, expert_half(): part = lax.ppermute(part, 'ep', [(d, d ^ mask) for d in range(ways)])  12.6 us
    ppermute x7, waiting for transfers between devices, expert_half(): part = lax.ppermute(part, 'ep', [(d, d ^ mask) for d in range(ways)])  10.1 us
    dot_general x1, matrix products, expert_half(): jnp.einsum('abecf,efd->abecd', hidden, expert_down, preferred_element_typ...  7.52 us
    all_to_all x1, blocking collectives, mixer_half(): lax.all_to_all(attended, 'tp', split_axis=0, concat_axis=1, tiled=True)  6.3 us
  transfers between devices with their start and end apart: 10, of which 3 were waited for; matrix products, arithmetic and copies ran while one was open for 2% of the time, Pallas kernels for 0%

profile of v1, /device:TPU:0, one launch (start us, length us, event | category | flops | bytes accessed | tf_op | source)
XLA Modules:
  0.0 171.6 jit_solution(7453408059214138154)
XLA Ops:
  7.3 0.9 constant_dynamic-slice_fusion.7
  8.2 0.1 eq.51
  8.5 0.2 reduce_window_sum.11
  8.7 0.2 select_reduce_fusion
  8.8 0.1 reduce_sum.48
  9.1 0.8 multiply_add_fusion
  9.9 1.1 fusion.18
  11.0 0.7 convert_element_type.68
  11.7 1.4 convolution_convert_fusion.1
  13.3 3.1 %collective-permute-start = (bf16[1,1,24,2048]{3,2,1,0:T(8,128)(2,1)S(1)}, bf16[1,1,24,2048]{3,2,1,0:T(8,128)(2,1)S(1)}, u32[]{:S(2)}, u32[]{:S(2)}) collective-permute-start(bf16[1,1,24,2048]{3,2,1,0:T(8,128)(2,1)S(1)} %get-tuple-element.111), channel_id=1, source_target_pairs={{0,4},{4,0},{8,12},{12,8},{16,20},{20,16},{24,28},{28,24},{1,5},{5... | collective-permute-start | bytes 294920 | tf_op jit(solution)/shard_map/ppermute | solution.py:109
  16.4 1.6 collective-permute-start.1
  17.9 3.0 %collective-permute-start.3 = (bf16[1,1,24,2048]{3,2,1,0:T(8,128)(2,1)S(1)}, bf16[1,1,24,2048]{3,2,1,0:T(8,128)(2,1)S(1)}, u32[]{:S(2)}, u32[]{:S(2)}) collective-permute-start(bf16[1,1,24,2048]{3,2,1,0:T(8,128)(2,1)S(1)} %get-tuple-element.108), channel_id=1, source_target_pairs={{0,16},{4,20},{8,24},{12,28},{16,0},{20,4},{24,8},{28,12},{1,17},{... | collective-permute-start | bytes 294920 | tf_op jit(solution)/shard_map/ppermute | solution.py:109
  20.9 1.3 collective-permute-start.4
  22.2 3.6 %collective-permute-start.5 = (bf16[1,1,24,2048]{3,2,1,0:T(8,128)(2,1)S(1)}, bf16[1,1,24,2048]{3,2,1,0:T(8,128)(2,1)S(1)}, u32[]{:S(2)}, u32[]{:S(2)}) collective-permute-start(bf16[1,1,24,2048]{3,2,1,0:T(8,128)(2,1)S(1)} %get-tuple-element.106), channel_id=1, source_target_pairs={{0,24},{4,28},{8,16},{12,20},{16,8},{20,12},{24,0},{28,4},{1,25},{... | collective-permute-start | bytes 294920 | tf_op jit(solution)/shard_map/ppermute | solution.py:109
  26.0 10.1 %collective-permute-done.4 = bf16[1,1,24,2048]{3,2,1,0:T(8,128)(2,1)S(1)} collective-permute-done((bf16[1,1,24,2048]{3,2,1,0:T(8,128)(2,1)S(1)}, bf16[1,1,24,2048]{3,2,1,0:T(8,128)(2,1)S(1)}, u32[]{:S(2)}, u32[]{:S(2)}) %collective-permute-start.4) | collective-permute-done | bytes 98336 | tf_op jit(solution)/shard_map/ppermute | solution.py:109
  36.2 0.9 copy-done.1
  37.2 30.4 %all-gather.2.cloned.1.call-done = bf16[4,8,24,2048]{3,2,1,0:T(8,128)(2,1)} async-done(((bf16[1,8,24,2048]{3,2,1,0:T(8,128)(2,1)}), bf16[4,8,24,2048]{3,2,1,0:T(8,128)(2,1)}) %all-gather.2.cloned.1.call-update) | async-done | bytes 3145744 | tf_op jit(solution)/shard_map/all_gather | solution.py:112
  67.5 4.0 %convolution_bitcast_fusion.1 = f32[4,8,1,24,256]{4,3,1,0,2:T(8,128)} fusion(bf16[4,8,24,2048]{3,2,1,0:T(8,128)(2,1)} %all-gather.2.cloned.1.call-done, bf16[1,2048,256]{2,1,0:T(8,128)(2,1)} %param.24), kind=kOutput, calls=%fused_computation.25 | convolution fusion | flops 805306368 | bytes 4980736 | tf_op jit(solution)/shard_map/abecd,edf->abecf/dot_general | solution.py:118
  71.6 7.5 %fusion.13 = bf16[4,8,1,24,2048]{4,3,1,0,2:T(8,128)(2,1)} fusion(bf16[1,256,2048]{2,1,0:T(8,128)(2,1)S(1)} %copy-done.6, f32[4,8,1,24,256]{4,3,1,0,2:T(8,128)} %convolution_bitcast_fusion.1, bf16[4,8,24,2048]{3,2,1,0:T(8,128)(2,1)} %all-gather.2.cloned.1.call-done, bf16[1,2048,256]{2,1,0:T(8,128)(2,1)} %param.23), kind=kOutput, calls=%fused_computation.21 | convolution fusion | flops 1613365248 | bytes 9175040 | tf_op jit(solution)/shard_map/abecf,efd->abecd/dot_general | solution.py:122
  79.1 0.7 copy-done.3
  79.8 26.2 %all_gather.10 = bf16[1,64,1024]{2,1,0:T(8,128)(2,1)S(1)} all-gather(bf16[1,64,128]{2,1,0:T(8,128)(2,1)S(1)} %copy-done.3), channel_id=1, replica_groups=mesh['ep'=8,'tp'=4] {'ep'}, dimensions={2}, use_global_device_ids=true | all-gather | bytes 147456 | tf_op jit(solution)/shard_map/all_gather | solution.py:40
  106.0 26.2 %all_gather.9 = bf16[1,64,1024]{2,1,0:T(8,128)(2,1)S(1)} all-gather(bf16[1,64,128]{2,1,0:T(8,128)(2,1)S(1)} %copy-done.4), channel_id=1, replica_groups=mesh['ep'=8,'tp'=4] {'ep'}, dimensions={2}, use_global_device_ids=true | all-gather | bytes 147456 | tf_op jit(solution)/shard_map/all_gather | solution.py:39
  132.2 1.2 conditional.1
  132.5 0.4 fusion.40
  132.9 0.2 fusion.7
  133.1 0.3 fusion.5
  133.4 0.1 copy.50
  133.5 6.3 %all_to_all.24 = bf16[4,32,128]{2,1,0:T(8,128)(2,1)S(1)} all-to-all(bf16[4,32,128]{2,1,0:T(8,128)(2,1)S(1)} %bitcast.126), channel_id=1, replica_groups=mesh['ep'=8,'tp'=4] {'tp'}, dimensions={0} | all-to-all | bytes 65536 | tf_op jit(solution)/shard_map/all_to_all | solution.py:76
  139.8 3.5 %all-to-all-start.1 = ((bf16[1,8,24,2048]{3,2,0,1:T(8,128)(2,1)}), bf16[1,8,24,2048]{3,2,0,1:T(8,128)(2,1)S(1)}, u32[]{:S(2)}, u32[]{:S(2)}) async-start(bf16[1,8,24,2048]{3,2,0,1:T(8,128)(2,1)} %bitcast.123), calls=%async_computation.2 | async-start | bytes 1572864 | tf_op jit(solution)/shard_map/all_to_all | solution.py:132
  143.5 1.1 convolution_convert_fusion.2
  144.6 19.1 %all-to-all-done.1 = bf16[1,8,24,2048]{3,2,0,1:T(8,128)(2,1)S(1)} async-done(((bf16[1,8,24,2048]{3,2,0,1:T(8,128)(2,1)}), bf16[1,8,24,2048]{3,2,0,1:T(8,128)(2,1)S(1)}, u32[]{:S(2)}, u32[]{:S(2)}) %all-to-all-start.1) | async-done | bytes 786464 | tf_op jit(solution)/shard_map/all_to_all | solution.py:132
  163.7 1.1 fusion.14
  (49 shorter events, 1.2 us)
Async XLA Ops:
  7.2 136.3 %copy-start = (bf16[512,2048]{1,0:T(8,128)(2,1)S(1)}, bf16[512,2048]{1,0:T(8,128)(2,1)}, u32[]{:S(2)}) copy-start(bf16[512,2048]{1,0:T(8,128)(2,1)} %param.18) | copy-start | bytes 6291460
  7.2 60.4 %all-gather.2.cloned.1.call-start = ((), (), s32[]{:S(2)}) async-start(), calls=%async_computation.3 | async-start | bytes 3932160 | tf_op jit(solution)/shard_map/all_gather | solution.py:112
  13.3 8.9 %collective-permute-start = (bf16[1,1,24,2048]{3,2,1,0:T(8,128)(2,1)S(1)}, bf16[1,1,24,2048]{3,2,1,0:T(8,128)(2,1)S(1)}, u32[]{:S(2)}, u32[]{:S(2)}) collective-permute-start(bf16[1,1,24,2048]{3,2,1,0:T(8,128)(2,1)S(1)} %get-tuple-element.111), channel_id=1, source_target_pairs={{0,4},{4,0},{8,12},{12,8},{16,20},{20,16},{24,28},{28,24},{1,5},{5... | collective-permute-start | bytes 294920 | tf_op jit(solution)/shard_map/ppermute | solution.py:109
  16.4 9.5 %collective-permute-start.1 = (bf16[1,1,24,2048]{3,2,1,0:T(8,128)(2,1)S(1)}, bf16[1,1,24,2048]{3,2,1,0:T(8,128)(2,1)S(1)}, u32[]{:S(2)}, u32[]{:S(2)}) collective-permute-start(bf16[1,1,24,2048]{3,2,1,0:T(8,128)(2,1)S(1)} %get-tuple-element.110), channel_id=1, source_target_pairs={{0,8},{4,12},{8,0},{12,4},{16,24},{20,28},{24,16},{28,20},{1,9},{5... | collective-permute-start | bytes 294920 | tf_op jit(solution)/shard_map/ppermute | solution.py:109
  17.9 8.0 %collective-permute-start.2 = (bf16[1,1,24,2048]{3,2,1,0:T(8,128)(2,1)S(1)}, bf16[1,1,24,2048]{3,2,1,0:T(8,128)(2,1)S(1)}, u32[]{:S(2)}, u32[]{:S(2)}) collective-permute-start(bf16[1,1,24,2048]{3,2,1,0:T(8,128)(2,1)S(1)} %get-tuple-element.109), channel_id=1, source_target_pairs={{0,12},{4,8},{8,4},{12,0},{16,28},{20,24},{24,20},{28,16},{1,13},{... | collective-permute-start | bytes 294920 | tf_op jit(solution)/shard_map/ppermute | solution.py:109
  17.9 8.0 %collective-permute-start.3 = (bf16[1,1,24,2048]{3,2,1,0:T(8,128)(2,1)S(1)}, bf16[1,1,24,2048]{3,2,1,0:T(8,128)(2,1)S(1)}, u32[]{:S(2)}, u32[]{:S(2)}) collective-permute-start(bf16[1,1,24,2048]{3,2,1,0:T(8,128)(2,1)S(1)} %get-tuple-element.108), channel_id=1, source_target_pairs={{0,16},{4,20},{8,24},{12,28},{16,0},{20,4},{24,8},{28,12},{1,17},{... | collective-permute-start | bytes 294920 | tf_op jit(solution)/shard_map/ppermute | solution.py:109
  20.9 15.2 %collective-permute-start.4 = (bf16[1,1,24,2048]{3,2,1,0:T(8,128)(2,1)S(1)}, bf16[1,1,24,2048]{3,2,1,0:T(8,128)(2,1)S(1)}, u32[]{:S(2)}, u32[]{:S(2)}) collective-permute-start(bf16[1,1,24,2048]{3,2,1,0:T(8,128)(2,1)S(1)} %get-tuple-element.107), channel_id=1, source_target_pairs={{0,20},{4,16},{8,28},{12,24},{16,4},{20,0},{24,12},{28,8},{1,21},{... | collective-permute-start | bytes 294920 | tf_op jit(solution)/shard_map/ppermute | solution.py:109
  22.2 13.9 %collective-permute-start.5 = (bf16[1,1,24,2048]{3,2,1,0:T(8,128)(2,1)S(1)}, bf16[1,1,24,2048]{3,2,1,0:T(8,128)(2,1)S(1)}, u32[]{:S(2)}, u32[]{:S(2)}) collective-permute-start(bf16[1,1,24,2048]{3,2,1,0:T(8,128)(2,1)S(1)} %get-tuple-element.106), channel_id=1, source_target_pairs={{0,24},{4,28},{8,16},{12,20},{16,8},{20,12},{24,0},{28,4},{1,25},{... | collective-permute-start | bytes 294920 | tf_op jit(solution)/shard_map/ppermute | solution.py:109
  25.8 10.3 %collective-permute-start.6 = (bf16[1,1,24,2048]{3,2,1,0:T(8,128)(2,1)S(1)}, bf16[1,1,24,2048]{3,2,1,0:T(8,128)(2,1)S(1)}, u32[]{:S(2)}, u32[]{:S(2)}) collective-permute-start(bf16[1,1,24,2048]{3,2,1,0:T(8,128)(2,1)S(1)} %get-tuple-element.105), channel_id=1, source_target_pairs={{0,28},{4,24},{8,20},{12,16},{16,12},{20,8},{24,4},{28,0},{1,29},{... | collective-permute-start | bytes 294920 | tf_op jit(solution)/shard_map/ppermute | solution.py:109
  36.2 0.9 copy-start.1
  37.1 34.5 %copy-start.6 = (bf16[1,256,2048]{2,1,0:T(8,128)(2,1)S(1)}, bf16[1,256,2048]{2,1,0:T(8,128)(2,1)}, u32[]{:S(2)}) copy-start(bf16[1,256,2048]{2,1,0:T(8,128)(2,1)} %param.25) | copy-start | bytes 3145732
  37.1 102.7 %reduce-scatter.2.cloned.1.call-start = ((), (), s32[]{:S(2)}) async-start(), calls=%async_computation.4 | async-start | bytes 3932160 | tf_op jit(solution)/shard_map/reduce_scatter | solution.py:126
  79.1 0.7 copy-start.3
  79.1 26.9 %copy-start.4 = (bf16[1,64,128]{2,1,0:T(8,128)(2,1)S(1)}, bf16[1,64,128]{2,1,0:T(8,128)(2,1)}, u32[]{:S(2)}) copy-start(bf16[1,64,128]{2,1,0:T(8,128)(2,1)} %param.15) | copy-start | bytes 49156
  79.1 53.1 %copy-start.2 = (bf16[128,128]{1,0:T(8,128)(2,1)S(1)}, bf16[128,128]{1,0:T(8,128)(2,1)}, u32[]{:S(2)}) copy-start(bf16[128,128]{1,0:T(8,128)(2,1)} %param.14) | copy-start | bytes 98308
  79.1 53.1 %copy-start.7 = (f32[1,1024]{1,0:T(1,128)S(1)}, f32[1,1024]{1,0:T(1,128)}, u32[]{:S(2)}) copy-start(f32[1,1024]{1,0:T(1,128)} %param.17) | copy-start | bytes 12292
  132.2 11.2 %copy-start.5 = (f32[256,2]{0,1:T(2,128)S(1)}, f32[256,2]{0,1:T(2,128)}, u32[]{:S(2)}) copy-start(f32[256,2]{0,1:T(2,128)} %param.22) | copy-start | bytes 6148
  139.8 23.8 %all-to-all-start.1 = ((bf16[1,8,24,2048]{3,2,0,1:T(8,128)(2,1)}), bf16[1,8,24,2048]{3,2,0,1:T(8,128)(2,1)S(1)}, u32[]{:S(2)}, u32[]{:S(2)}) async-start(bf16[1,8,24,2048]{3,2,0,1:T(8,128)(2,1)} %bitcast.123), calls=%async_computation.2 | async-start | bytes 1572864 | tf_op jit(solution)/shard_map/all_to_all | solution.py:132
Sparse Core Ops, SparseCore 0:
  37.2 30.2 all-gather.1
  79.2 37.8 reduce-scatter.1
